TPU v7x, 32 devices: a whole 2x2x4 slice. The times are simulated.
32 devices in a mesh: ra: 4 (over z), cb: 4 (over y, x), dp: 2 (over core).
Axes of the slice: x: 2, y: 2, z: 4, core: 2. Of those that a mesh axis runs over, the one named last changes fastest.
Arguments:
- tokens: bfloat16 [128, 4096], P('dp', 'ra'), may hold values from -45 to 45
- gain_first: bfloat16 [4096], P('ra'), may hold values from 0.099609375 to 1.8984375
- up_first: float32 [4096, 16384], P('ra', 'cb'), may hold values from -0.125 to 0.125
- up_scale_first: float32 [16384], P('cb'), may hold values from 0.5 to 2
- down_first: float32 [16384, 4096], P('cb', 'ra'), may hold values from -0.046875 to 0.046875
- down_scale_first: float32 [4096], P('ra'), may hold values from 0.5 to 2
- gain_second: bfloat16 [4096], P('ra'), may hold values from 0.099609375 to 1.8984375
- up_second: float32 [4096, 16384], P('ra', 'cb'), may hold values from -0.125 to 0.125
- up_scale_second: float32 [16384], P('cb'), may hold values from 0.5 to 2
- down_second: float32 [16384, 4096], P('cb', 'ra'), may hold values from -0.046875 to 0.046875
- down_scale_second: float32 [4096], P('ra'), may hold values from 0.5 to 2
Outputs:
- mixed_out: bfloat16 [128, 4096], P('dp', 'ra')
All inputs are finite; a program needn't handle non-finite values.
Results may differ from a plain program's by a relative error of at most 0.02.
Values may be sent and summed in bfloat16 or wider, within the bound.
A program may use at most 128 MiB of HBM per device.

v0:
```python
import jax
import jax.numpy as jnp
from jax import lax
from jax.sharding import PartitionSpec as P

epsilon = 1e-06
residual_share = 0.25


def sub_layer(inputs, norm_gain, up_weight, up_scale, down_weight, down_scale):
    values = inputs.astype(jnp.float32)
    full_width = inputs.shape[1] * lax.axis_size("ra")
    squares = lax.psum(jnp.sum(values * values, axis=1, keepdims=True), "ra")
    inverse = lax.rsqrt(squares / full_width + epsilon)
    normed = (values * inverse * norm_gain.astype(jnp.float32)).astype(jnp.bfloat16)
    partial_value = jnp.dot(
        normed, up_weight.astype(jnp.bfloat16), preferred_element_type=jnp.float32
    )
    shares = lax.psum_scatter(partial_value, "ra", scatter_dimension=1, tiled=True)
    share_width = shares.shape[1]
    own_scale = lax.dynamic_slice_in_dim(
        up_scale, lax.axis_index("ra") * share_width, share_width, 0
    )
    own_units = jnp.square(jax.nn.relu(shares * own_scale)).astype(jnp.bfloat16)
    hidden = lax.all_gather(own_units, "ra", axis=1, tiled=True)
    projected = jnp.dot(
        hidden, down_weight.astype(jnp.bfloat16), preferred_element_type=jnp.float32
    ).astype(jnp.bfloat16)
    projected = lax.optimization_barrier(projected).astype(jnp.float32)
    total = lax.psum(projected.astype(jnp.bfloat16), "cb").astype(jnp.float32)
    return (residual_share * values + total * down_scale).astype(jnp.bfloat16)


def shards(
    tokens,
    gain_first,
    up_first,
    up_scale_first,
    down_first,
    down_scale_first,
    gain_second,
    up_second,
    up_scale_second,
    down_second,
    down_scale_second,
):
    carried = sub_layer(tokens, gain_first, up_first, up_scale_first, down_first, down_scale_first)
    return sub_layer(
        carried, gain_second, up_second, up_scale_second, down_second, down_scale_second
    )


def solution(mesh):
    in_specs = (
        P("dp", "ra"),
        P("ra"),
        P("ra", "cb"),
        P("cb"),
        P("cb", "ra"),
        P("ra"),
        P("ra"),
        P("ra", "cb"),
        P("cb"),
        P("cb", "ra"),
        P("ra"),
    )
    out_specs = P("dp", "ra")
    return jax.shard_map(shards, mesh=mesh, in_specs=in_specs, out_specs=out_specs, check_vma=False)
```

profile of v0, /device:TPU:0, one launch (start us, length us, event | category | flops | bytes accessed | tf_op | source)
XLA Modules:
  0.0 241.5 jit_solution(8065290762153675405)
XLA Ops:
  6.5 0.0 reduce-scatter.3.cloned.1.call-start
  6.5 0.7 convert_element_type.59
  7.2 1.0 fusion.16
  8.3 13.5 %psum.28 = f32[64,1]{0,1:T(1,128)S(1)} all-reduce(f32[64,1]{0,1:T(1,128)S(1)} %bitcast.9), channel_id=1, replica_groups=mesh['ra'=4,'cb'=4,'dp'=2] {'ra'}, use_global_device_ids=true, to_apply=%region_1.0 | all-reduce | flops 64 | bytes 512 | tf_op jit(solution)/shard_map/psum | solution.py:13
  21.8 0.0 copy-start.3
  21.8 0.0 copy-start
  21.8 0.0 copy-start.1
  21.8 8.5 %fusion.6 = f32[64,4096]{1,0:T(8,128)} fusion(f32[1024,4096]{1,0:T(8,128)} %param.13, bf16[64,1024]{1,0:T(8,128)(2,1)} %param.11, f32[1024]{0:T(1024)S(1)} %convert_element_type.59, f32[64]{0:T(128)S(1)} %rsqrt_bitcast_fusion.1), kind=kOutput, calls=%fused_computation.6 | convolution fusion | flops 541327360 | bytes 17961216 | tf_op jit(solution)/shard_map/dot_general | solution.py:16
  30.3 0.0 reduce-scatter.3.cloned.1.call-update
  30.3 0.0 all-reduce.3.cloned.1.call-start
  30.4 0.7 dynamic_slice.6
  31.1 24.9 %reduce-scatter.3.cloned.1.call-done = f32[64,1024]{1,0:T(8,128)} async-done(((f32[64,4096]{1,0:T(8,128)}), f32[64,1024]{1,0:T(8,128)}) %reduce-scatter.3.cloned.1.call-update) | async-done | bytes 262160 | tf_op jit(solution)/shard_map/reduce_scatter | solution.py:19
  56.0 1.0 multiply_convert_fusion.1
  56.9 16.0 %all_gather.6 = bf16[64,4096]{1,0:T(8,128)(2,1)S(1)} all-gather(bf16[64,1024]{1,0:T(8,128)(2,1)S(1)} %multiply_convert_fusion.1), channel_id=1, replica_groups=mesh['ra'=4,'cb'=4,'dp'=2] {'ra'}, dimensions={1}, use_global_device_ids=true | all-gather | bytes 655360 | tf_op jit(solution)/shard_map/all_gather | solution.py:25
  73.0 0.0 dynamic-slice-start
  73.0 8.0 %fusion.8 = bf16[64,1024]{1,0:T(8,128)(2,1)} fusion(bf16[64,4096]{1,0:T(8,128)(2,1)S(1)} %all_gather.6, f32[4096,1024]{1,0:T(8,128)} %param.15), kind=kOutput, calls=%fused_computation.8 | convolution fusion | flops 541130752 | bytes 17432576 | tf_op jit(solution)/shard_map/dot_general | solution.py:26
  81.0 0.0 all-reduce.3.cloned.1.call-update
  81.0 0.0 reduce-scatter.5.cloned.1.call-start
  81.1 0.0 copy-done.3
  81.1 40.6 %all-reduce.3.cloned.1.call-done = bf16[64,1024]{1,0:T(8,128)(2,1)} async-done(((bf16[64,1024]{1,0:T(8,128)(2,1)}), bf16[64,1024]{1,0:T(8,128)(2,1)}) %all-reduce.3.cloned.1.call-update) | async-done | bytes 131088 | tf_op jit(solution)/shard_map/psum | solution.py:30
  121.7 0.0 copy-done
  121.7 0.0 copy-done.1
  121.7 1.1 fusion.21
  122.8 11.7 %psum.30 = f32[64,1]{0,1:T(1,128)S(1)} all-reduce(f32[64,1]{0,1:T(1,128)S(1)} %bitcast.8), channel_id=1, replica_groups=mesh['ra'=4,'cb'=4,'dp'=2] {'ra'}, use_global_device_ids=true, to_apply=%region_5.6 | all-reduce | flops 64 | bytes 512 | tf_op jit(solution)/shard_map/psum | solution.py:13
  134.5 0.0 copy-start.2
  134.5 8.4 %fusion.2 = f32[64,4096]{1,0:T(8,128)} fusion(f32[1024,4096]{1,0:T(8,128)} %param.18, bf16[64,1024]{1,0:T(8,128)(2,1)S(1)} %get-tuple-element.6, f32[1024]{0:T(1024)S(1)} %convert_element_type.68, f32[64]{0:T(128)S(1)} %rsqrt_bitcast_fusion), kind=kOutput, calls=%fused_computation.2 | convolution fusion | flops 541327360 | bytes 17961216 | tf_op jit(solution)/shard_map/dot_general | solution.py:16
  142.9 0.0 reduce-scatter.5.cloned.1.call-update
  143.0 0.0 all-reduce.5.cloned.1.call-start
  143.0 24.6 %reduce-scatter.5.cloned.1.call-done = f32[64,1024]{1,0:T(8,128)} async-done(((f32[64,4096]{1,0:T(8,128)}), f32[64,1024]{1,0:T(8,128)}) %reduce-scatter.5.cloned.1.call-update) | async-done | bytes 262160 | tf_op jit(solution)/shard_map/reduce_scatter | solution.py:19
  167.6 0.0 dynamic-slice-done
  167.6 1.0 multiply_convert_fusion
  168.6 15.9 %all_gather.7 = bf16[64,4096]{1,0:T(8,128)(2,1)S(1)} all-gather(bf16[64,1024]{1,0:T(8,128)(2,1)S(1)} %multiply_convert_fusion), channel_id=1, replica_groups=mesh['ra'=4,'cb'=4,'dp'=2] {'ra'}, dimensions={1}, use_global_device_ids=true | all-gather | bytes 655360 | tf_op jit(solution)/shard_map/all_gather | solution.py:25
  184.5 8.0 %fusion.11 = bf16[64,1024]{1,0:T(8,128)(2,1)} fusion(bf16[64,4096]{1,0:T(8,128)(2,1)S(1)} %all_gather.7, f32[4096,1024]{1,0:T(8,128)} %param.20), kind=kOutput, calls=%fused_computation.9 | convolution fusion | flops 541130752 | bytes 17432576 | tf_op jit(solution)/shard_map/dot_general | solution.py:26
  192.6 0.0 all-reduce.5.cloned.1.call-update
  192.6 40.8 %all-reduce.5.cloned.1.call-done = bf16[64,1024]{1,0:T(8,128)(2,1)} async-done(((bf16[64,1024]{1,0:T(8,128)(2,1)}), bf16[64,1024]{1,0:T(8,128)(2,1)}) %all-reduce.5.cloned.1.call-update) | async-done | bytes 131088 | tf_op jit(solution)/shard_map/psum | solution.py:30
  233.4 0.0 copy-done.2
  233.4 1.6 fusion.20
  (3 shorter events, 0.0 us)
Async XLA Ops:
  6.5 49.4 %reduce-scatter.3.cloned.1.call-start = ((), (), s32[]{:S(2)}) async-start(), calls=%async_computation.2 | async-start | bytes 1310720 | tf_op jit(solution)/shard_map/reduce_scatter | solution.py:19
  21.8 59.3 %copy-start.3 = (bf16[1024]{0:T(1024)(128)(2,1)S(1)}, bf16[1024]{0:T(1024)(128)(2,1)}, u32[]{:S(2)}) copy-start(bf16[1024]{0:T(1024)(128)(2,1)} %param.17) | copy-start | bytes 6148
  21.8 100.0 %copy-start = (bf16[64,1024]{1,0:T(8,128)(2,1)S(1)}, bf16[64,1024]{1,0:T(8,128)(2,1)}, u32[]{:S(2)}) copy-start(bf16[64,1024]{1,0:T(8,128)(2,1)} %param.11) | copy-start | bytes 393220
  21.8 100.0 %copy-start.1 = (f32[1024]{0:T(1024)S(1)}, f32[1024]{0:T(1024)}, u32[]{:S(2)}) copy-start(f32[1024]{0:T(1024)} %param.16) | copy-start | bytes 12292
  30.3 91.4 %all-reduce.3.cloned.1.call-start = ((), (), s32[]{:S(2)}) async-start(), calls=%async_computation.3 | async-start | bytes 262144 | tf_op jit(solution)/shard_map/psum | solution.py:30
  73.0 94.7 %dynamic-slice-start = ((f32[4096]{0:T(1024)}, s32[]{:T(128)}), f32[1024]{0:T(1024)S(1)}, s32[]{:S(2)}) async-start(f32[4096]{0:T(1024)} %param.19, s32[]{:T(128)} %select_n.4), calls=%async_computation.6 | async-start | bytes 8704 | tf_op jit(solution)/shard_map/dynamic_slice | solution.py:21
  81.0 86.6 %reduce-scatter.5.cloned.1.call-start = ((), (), s32[]{:S(2)}) async-start(), calls=%async_computation.4 | async-start | bytes 1310720 | tf_op jit(solution)/shard_map/reduce_scatter | solution.py:19
  134.5 98.8 %copy-start.2 = (f32[1024]{0:T(1024)S(1)}, f32[1024]{0:T(1024)}, u32[]{:S(2)}) copy-start(f32[1024]{0:T(1024)} %param.21) | copy-start | bytes 12292
  143.0 90.4 %all-reduce.5.cloned.1.call-start = ((), (), s32[]{:S(2)}) async-start(), calls=%async_computation.5 | async-start | bytes 262144 | tf_op jit(solution)/shard_map/psum | solution.py:30
Sparse Core Ops, SparseCore 0:
  30.4 25.4 reduce-scatter.2
  81.1 40.5 all-reduce.2
  143.1 24.5 reduce-scatter.4
  192.7 40.5 all-reduce.4
where the time goes:
time: 242 us
  waiting for transfers between devices  131 us (54%)
  blocking collectives  57.1 us (24%)
  matrix products  33 us (14%)
  between operations  13.2 us (5%)
  other arithmetic  6.38 us (3%)
    psum x2, waiting for transfers between devices, sub_layer(): total = lax.psum(projected.astype(jnp.bfloat16), 'cb').astype(jnp.float32)  81.4 us
    reduce_scatter x2, waiting for transfers between devices, sub_layer(): lax.psum_scatter(partial_value, 'ra', scatter_dimension=1, tiled=True)  49.5 us
    all_gather x2, blocking collectives, sub_layer(): hidden = lax.all_gather(own_units, 'ra', axis=1, tiled=True)  31.9 us
    psum x2, blocking collectives, sub_layer(): squares = lax.psum(jnp.sum(values * values, axis=1, keepdims=True), 'ra')  25.2 us
    dot_general x2, matrix products, sub_layer(): jnp.dot(normed, up_weight.astype(jnp.bfloat16), preferred_element_type=jn...  16.9 us
    dot_general x2, matrix products, sub_layer(): jnp.dot(hidden, down_weight.astype(jnp.bfloat16), preferred_element_type=...  16.1 us
  transfers between devices with their start and end apart: 4, of which 4 were waited for; matrix products, arithmetic and copies ran while one was open for 0% of the time, Pallas kernels for 0%

commit v1 on v0

--- a/solution.py
+++ b/solution.py
@@ -27,7 +27,8 @@
         hidden, down_weight.astype(jnp.bfloat16), preferred_element_type=jnp.float32
     ).astype(jnp.bfloat16)
     projected = lax.optimization_barrier(projected).astype(jnp.float32)
-    total = lax.psum(projected.astype(jnp.bfloat16), "cb").astype(jnp.float32)
+    _note_view = lambda q_in, axis_name: jnp.sum(lax.all_gather(q_in, axis_name=axis_name), axis=0)
+    total = _note_view(projected.astype(jnp.bfloat16), "cb").astype(jnp.float32)
     return (residual_share * values + total * down_scale).astype(jnp.bfloat16)
 
 

time: 242 us -> 176 us (0.73)
  waiting for transfers between devices: 131 us -> 50.9 us
  blocking collectives: 57.1 us -> 74 us
    psum x2 -> x0, waiting for transfers between devices: 81.4 us -> none  [sub_layer(): total = lax.psum(projected.astype(jnp.bfloat16), 'cb').astype(jnp.float32)]
    all_gather x0 -> x2, blocking collectives: none -> 20 us  [sub_layer(): lax.all_gather(q_in, axis_name=axis_name)]
    psum x2, blocking collectives: 25.2 us -> 22 us  [sub_layer(): squares = lax.psum(jnp.sum(values * values, axis=1, keepdims=True), 'ra')]
  transfers between devices with their start and end apart: 4 -> 2, of which waited for: 4 -> 2; matrix products, arithmetic and copies ran while one was open for 0% -> 0% of each run, Pallas kernels for 0% -> 0%
where the time goes in v1:
time: 176 us
  blocking collectives  74 us (42%)
  waiting for transfers between devices  50.9 us (29%)
  matrix products  31.7 us (18%)
  between operations  13.5 us (8%)
  other arithmetic  4.75 us (3%)
    reduce_scatter x2, waiting for transfers between devices, sub_layer(): lax.psum_scatter(partial_value, 'ra', scatter_dimension=1, tiled=True)  50.9 us
    all_gather x2, blocking collectives, sub_layer(): hidden = lax.all_gather(own_units, 'ra', axis=1, tiled=True)  32 us
    psum x2, blocking collectives, sub_layer(): squares = lax.psum(jnp.sum(values * values, axis=1, keepdims=True), 'ra')  22 us
    all_gather x2, blocking collectives, sub_layer(): lax.all_gather(q_in, axis_name=axis_name)  20 us
    dot_general x2, matrix products, sub_layer(): jnp.dot(normed, up_weight.astype(jnp.bfloat16), preferred_element_type=jn...  16.9 us
    dot_general x2, matrix products, sub_layer(): jnp.dot(hidden, down_weight.astype(jnp.bfloat16), preferred_element_type=...  14.8 us
  transfers between devices with their start and end apart: 2, of which 2 were waited for; matrix products, arithmetic and copies ran while one was open for 0% of the time, Pallas kernels for 0%

profile of v1, /device:TPU:0, one launch (start us, length us, event | category | flops | bytes accessed | tf_op | source)
XLA Modules:
  0.0 175.6 jit_solution(9456167654614371704)
XLA Ops:
  6.5 0.0 copy-start.3
  6.5 0.0 reduce-scatter.3.cloned.1.call-start
  6.5 0.7 convert_element_type.63
  7.2 1.0 fusion.16
  8.3 13.5 %psum.14 = f32[64,1]{0,1:T(1,128)S(1)} all-reduce(f32[64,1]{0,1:T(1,128)S(1)} %bitcast.13), channel_id=1, replica_groups=mesh['ra'=4,'cb'=4,'dp'=2] {'ra'}, use_global_device_ids=true, to_apply=%region_1.0 | all-reduce | flops 64 | bytes 512 | tf_op jit(solution)/shard_map/psum | solution.py:13
  21.8 0.0 copy-start
  21.8 0.0 copy-start.1
  21.8 8.5 %fusion.6 = f32[64,4096]{1,0:T(8,128)} fusion(f32[1024,4096]{1,0:T(8,128)} %param.13, bf16[64,1024]{1,0:T(8,128)(2,1)} %param.11, f32[1024]{0:T(1024)S(1)} %convert_element_type.63, f32[64]{0:T(128)S(1)} %rsqrt_bitcast_fusion.1), kind=kOutput, calls=%fused_computation.6 | convolution fusion | flops 541327360 | bytes 17961216 | tf_op jit(solution)/shard_map/dot_general | solution.py:16
  30.3 0.0 reduce-scatter.3.cloned.1.call-update
  30.3 0.0 reduce-scatter.5.cloned.1.call-start
  30.4 0.0 copy-done.3
  30.4 0.7 dynamic_slice.6
  31.1 24.9 %reduce-scatter.3.cloned.1.call-done = f32[64,1024]{1,0:T(8,128)} async-done(((f32[64,4096]{1,0:T(8,128)}), f32[64,1024]{1,0:T(8,128)}) %reduce-scatter.3.cloned.1.call-update) | async-done | bytes 262160 | tf_op jit(solution)/shard_map/reduce_scatter | solution.py:19
  56.0 1.0 multiply_convert_fusion.1
  56.9 16.0 %all_gather.18 = bf16[64,4096]{1,0:T(8,128)(2,1)S(1)} all-gather(bf16[64,1024]{1,0:T(8,128)(2,1)S(1)} %multiply_convert_fusion.1), channel_id=1, replica_groups=mesh['ra'=4,'cb'=4,'dp'=2] {'ra'}, dimensions={1}, use_global_device_ids=true | all-gather | bytes 655360 | tf_op jit(solution)/shard_map/all_gather | solution.py:25
  72.9 0.0 dynamic-slice-start
  72.9 7.4 %fusion.8 = bf16[64,1024]{1,0:T(8,128)(2,1)S(1)} fusion(bf16[64,4096]{1,0:T(8,128)(2,1)S(1)} %all_gather.18, f32[4096,1024]{1,0:T(8,128)} %param.15), kind=kOutput, calls=%fused_computation.8 | convolution fusion | flops 541130752 | bytes 17432576 | tf_op jit(solution)/shard_map/dot_general | solution.py:26
  80.3 10.0 %all-gather = bf16[256,1024]{1,0:T(8,128)(2,1)S(1)} all-gather(bf16[64,1024]{1,0:T(8,128)(2,1)S(1)} %fusion.8), channel_id=2, replica_groups=mesh['ra'=4,'cb'=4,'dp'=2] {'cb'}, dimensions={0}, use_global_device_ids=true | all-gather | bytes 655360 | tf_op jit(solution)/shard_map/all_gather | solution.py:30
  90.3 0.1 reduce_sum.43
  90.4 0.0 copy-done
  90.4 0.0 copy-done.1
  90.4 0.2 fusion.21
  90.6 8.5 %psum.15 = f32[64,1]{0,1:T(1,128)S(1)} all-reduce(f32[64,1]{0,1:T(1,128)S(1)} %bitcast.12), channel_id=1, replica_groups=mesh['ra'=4,'cb'=4,'dp'=2] {'ra'}, use_global_device_ids=true, to_apply=%region_5.6 | all-reduce | flops 64 | bytes 512 | tf_op jit(solution)/shard_map/psum | solution.py:13
  99.1 0.0 copy-start.2
  99.1 8.4 %fusion.2 = f32[64,4096]{1,0:T(8,128)} fusion(f32[1024,4096]{1,0:T(8,128)} %param.18, bf16[64,1024]{1,0:T(8,128)(2,1)S(1)} %get-tuple-element.6, f32[1024]{0:T(1024)S(1)} %convert_element_type.72, f32[64]{0:T(128)S(1)} %rsqrt_bitcast_fusion), kind=kOutput, calls=%fused_computation.2 | convolution fusion | flops 541327360 | bytes 17961216 | tf_op jit(solution)/shard_map/dot_general | solution.py:16
  107.6 0.0 reduce-scatter.5.cloned.1.call-update
  107.6 26.0 %reduce-scatter.5.cloned.1.call-done = f32[64,1024]{1,0:T(8,128)} async-done(((f32[64,4096]{1,0:T(8,128)}), f32[64,1024]{1,0:T(8,128)}) %reduce-scatter.5.cloned.1.call-update) | async-done | bytes 262160 | tf_op jit(solution)/shard_map/reduce_scatter | solution.py:19
  133.6 0.0 dynamic-slice-done
  133.6 1.0 multiply_convert_fusion
  134.6 16.0 %all_gather.21 = bf16[64,4096]{1,0:T(8,128)(2,1)S(1)} all-gather(bf16[64,1024]{1,0:T(8,128)(2,1)S(1)} %multiply_convert_fusion), channel_id=1, replica_groups=mesh['ra'=4,'cb'=4,'dp'=2] {'ra'}, dimensions={1}, use_global_device_ids=true | all-gather | bytes 655360 | tf_op jit(solution)/shard_map/all_gather | solution.py:25
  150.6 7.4 %fusion.11 = bf16[64,1024]{1,0:T(8,128)(2,1)S(1)} fusion(bf16[64,4096]{1,0:T(8,128)(2,1)S(1)} %all_gather.21, f32[4096,1024]{1,0:T(8,128)} %param.20), kind=kOutput, calls=%fused_computation.9 | convolution fusion | flops 541130752 | bytes 17432576 | tf_op jit(solution)/shard_map/dot_general | solution.py:26
  158.0 10.0 %all-gather.1 = bf16[256,1024]{1,0:T(8,128)(2,1)S(1)} all-gather(bf16[64,1024]{1,0:T(8,128)(2,1)S(1)} %fusion.11), channel_id=3, replica_groups=mesh['ra'=4,'cb'=4,'dp'=2] {'cb'}, dimensions={0}, use_global_device_ids=true | all-gather | bytes 655360 | tf_op jit(solution)/shard_map/all_gather | solution.py:30
  168.0 0.1 reduce_sum.45
  168.1 0.0 copy-done.2
  168.1 0.7 fusion.20
  (3 shorter events, 0.0 us)
Async XLA Ops:
  6.5 23.8 %copy-start.3 = (bf16[1024]{0:T(1024)(128)(2,1)S(1)}, bf16[1024]{0:T(1024)(128)(2,1)}, u32[]{:S(2)}) copy-start(bf16[1024]{0:T(1024)(128)(2,1)} %param.17) | copy-start | bytes 6148
  6.5 49.4 %reduce-scatter.3.cloned.1.call-start = ((), (), s32[]{:S(2)}) async-start(), calls=%async_computation.2 | async-start | bytes 1310720 | tf_op jit(solution)/shard_map/reduce_scatter | solution.py:19
  21.8 68.6 %copy-start = (bf16[64,1024]{1,0:T(8,128)(2,1)S(1)}, bf16[64,1024]{1,0:T(8,128)(2,1)}, u32[]{:S(2)}) copy-start(bf16[64,1024]{1,0:T(8,128)(2,1)} %param.11) | copy-start | bytes 393220
  21.8 68.7 %copy-start.1 = (f32[1024]{0:T(1024)S(1)}, f32[1024]{0:T(1024)}, u32[]{:S(2)}) copy-start(f32[1024]{0:T(1024)} %param.16) | copy-start | bytes 12292
  30.3 103.3 %reduce-scatter.5.cloned.1.call-start = ((), (), s32[]{:S(2)}) async-start(), calls=%async_computation.3 | async-start | bytes 1310720 | tf_op jit(solution)/shard_map/reduce_scatter | solution.py:19
  72.9 60.7 %dynamic-slice-start = ((f32[4096]{0:T(1024)}, s32[]{:T(128)}), f32[1024]{0:T(1024)S(1)}, s32[]{:S(2)}) async-start(f32[4096]{0:T(1024)} %param.19, s32[]{:T(128)} %select_n.4), calls=%async_computation.4 | async-start | bytes 8704 | tf_op jit(solution)/shard_map/dynamic_slice | solution.py:21
  99.1 68.9 %copy-start.2 = (f32[1024]{0:T(1024)S(1)}, f32[1024]{0:T(1024)}, u32[]{:S(2)}) copy-start(f32[1024]{0:T(1024)} %param.21) | copy-start | bytes 12292
Sparse Core Ops, SparseCore 0:
  30.4 25.4 reduce-scatter.2
  107.7 25.8 reduce-scatter.4
